TPU v7x, 32 devices: a whole 2x2x4 slice. The times are simulated.
32 devices in a mesh: grp: 2 (over y), ra: 4 (over z), cb: 4 (over x, core).
Axes of the slice: x: 2, y: 2, z: 4, core: 2. Of those that a mesh axis runs over, the one named last changes fastest.
Arguments:
- residual: bfloat16 [512, 4096], P('grp', 'ra'), parts along dimension 0, may hold values from -6 to 6
- gain_first: bfloat16 [4096], P('ra'), may hold values from 0.099609375 to 1.8984375
- gate_first: bfloat16 [4096, 11264], P('ra', 'cb'), may hold values from -0.09375 to 0.09375
- up_first: bfloat16 [4096, 11264], P('ra', 'cb'), may hold values from -0.09375 to 0.09375
- down_first: bfloat16 [11264, 4096], P('cb', 'ra'), may hold values from -0.078125 to 0.078125
- gain_second: bfloat16 [4096], P('ra'), may hold values from 0.099609375 to 1.8984375
- gate_second: bfloat16 [4096, 11264], P('ra', 'cb'), may hold values from -0.09375 to 0.09375
- up_second: bfloat16 [4096, 11264], P('ra', 'cb'), may hold values from -0.09375 to 0.09375
- down_second: bfloat16 [11264, 4096], P('cb', 'ra'), may hold values from -0.078125 to 0.078125
Outputs:
- updated: bfloat16 [512, 4096], P('grp', 'ra'), parts along dimension 0
There are 2 independent parts, one for each index of `grp`. A program takes and returns all parts, laid end to end along the dimension named above; an argument that names none is the same for every part. Nothing has to cross between parts.
All inputs are finite; a program needn't handle non-finite values.
Results may differ from a plain program's by a relative error of at most 0.0071.
Values may be sent and summed in bfloat16 or wider, within the bound.
A program may use at most 128 MiB of HBM per device.

v0:
```python
import jax
import jax.numpy as jnp
from jax import lax
from jax.sharding import PartitionSpec as P

D = 4096
epsilon = 1e-06


def half_step(stream, gain, w_gate, w_up, w_down):
    values = stream.astype(jnp.float32)
    square_part = jnp.sum(values * values, axis=1, keepdims=True)
    normed = (values * gain.astype(jnp.float32)).astype(jnp.bfloat16)
    gate_part = jnp.dot(normed, w_gate, preferred_element_type=jnp.float32)
    up_part = jnp.dot(normed, w_up, preferred_element_type=jnp.float32)
    gate_sum, up_sum, square_sum = (
        lax.psum_scatter(gate_part, "ra", scatter_dimension=0, tiled=True),
        lax.psum_scatter(up_part, "ra", scatter_dimension=0, tiled=True),
        lax.psum_scatter(square_part, "ra", scatter_dimension=0, tiled=True),
    )
    scale = lax.rsqrt(square_sum / D + epsilon)
    hidden = (jax.nn.silu(scale * gate_sum) * (scale * up_sum)).astype(jnp.bfloat16)
    down_part = jnp.dot(
        lax.all_gather(hidden, "ra", axis=0, tiled=True), w_down, preferred_element_type=jnp.float32
    )
    branch = lax.psum(down_part, "cb")
    return (values + 0.5 * branch).astype(jnp.bfloat16)


def per_device(
    residual,
    gain_first,
    gate_first,
    up_first,
    down_first,
    gain_second,
    gate_second,
    up_second,
    down_second,
):
    middle = half_step(residual, gain_first, gate_first, up_first, down_first)
    return half_step(middle, gain_second, gate_second, up_second, down_second)


def solution(mesh):
    in_specs = (
        P("grp", "ra"),
        P("ra"),
        P("ra", "cb"),
        P("ra", "cb"),
        P("cb", "ra"),
        P("ra"),
        P("ra", "cb"),
        P("ra", "cb"),
        P("cb", "ra"),
    )
    out_specs = P("grp", "ra")
    return jax.shard_map(
        per_device, mesh=mesh, in_specs=in_specs, out_specs=out_specs, check_vma=False
    )
```

profile of v0, /device:TPU:0, one launch (start us, length us, event | category | flops | bytes accessed | tf_op | source)
XLA Modules:
  0.0 450.0 jit_solution(18293002607253876413)
XLA Ops:
  6.5 1.2 fusion
  7.8 0.8 copy.10
  8.6 0.0 reduce-scatter.13.cloned.1.call-start
  8.6 0.7 convert_element_type.31
  9.3 6.1 %fusion.10 = f32[256,2816]{1,0:T(8,128)} fusion(bf16[1024,2816]{1,0:T(8,128)(2,1)} %param.12, bf16[256,1024]{1,0:T(8,128)(2,1)} %param.9, f32[1024]{0:T(1024)S(1)} %convert_element_type.31), kind=kOutput, calls=%fused_computation.16 | convolution fusion | flops 1477181440 | bytes 9179136 | tf_op jit(solution)/shard_map/dot_general | solution.py:15
  15.4 0.0 reduce-scatter.11.cloned.1.call-start
  15.5 5.9 %fusion.12 = f32[256,2816]{1,0:T(8,128)} fusion(bf16[1024,2816]{1,0:T(8,128)(2,1)} %param.11, bf16[256,1024]{1,0:T(8,128)(2,1)S(1)} %copy-done, f32[1024]{0:T(1024)S(1)} %convert_element_type.31), kind=kOutput, calls=%fused_computation.17 | convolution fusion | flops 1477181440 | bytes 9179136 | tf_op jit(solution)/shard_map/dot_general | solution.py:14
  21.5 0.0 all-gather.3.cloned.1.call-start
  21.5 10.3 %reduce-scatter.19.cloned.1.call-done = f32[64,1]{1,0:T(8,128)} async-done(((f32[256,1]{1,0:T(8,128)}), f32[64,1]{1,0:T(8,128)}) %reduce-scatter.19.cloned.1.call-update) | async-done | bytes 272
  31.8 0.8 add_rsqrt_fusion.1
  32.5 0.1 copy.14
  32.6 56.0 %reduce-scatter.13.cloned.1.call-done = f32[64,2816]{1,0:T(8,128)} async-done(((f32[256,2816]{1,0:T(8,128)}), f32[64,2816]{1,0:T(8,128)}) %reduce-scatter.13.cloned.1.call-update) | async-done | bytes 720912 | tf_op jit(solution)/shard_map/reduce_scatter | solution.py:18
  88.6 58.4 %reduce-scatter.11.cloned.1.call-done = f32[64,2816]{1,0:T(8,128)} async-done(((f32[256,2816]{1,0:T(8,128)}), f32[64,2816]{1,0:T(8,128)}) %reduce-scatter.11.cloned.1.call-update) | async-done | bytes 720912 | tf_op jit(solution)/shard_map/reduce_scatter | solution.py:17
  147.0 2.3 multiply_convert_fusion.1
  149.4 34.6 %all-gather.3.cloned.1.call-done = bf16[256,2816]{1,0:T(8,128)(2,1)} async-done(((bf16[64,2816]{1,0:T(8,128)(2,1)}), bf16[256,2816]{1,0:T(8,128)(2,1)}) %all-gather.3.cloned.1.call-update) | async-done | bytes 1441808 | tf_op jit(solution)/shard_map/all_gather | solution.py:24
  184.1 5.7 %fusion.15 = f32[256,1024]{1,0:T(8,128)} fusion(bf16[256,2816]{1,0:T(8,128)(2,1)} %all-gather.3.cloned.1.call-done, bf16[2816,1024]{1,0:T(8,128)(2,1)} %param.13), kind=kOutput, calls=%fused_computation.20 | convolution fusion | flops 1476395008 | bytes 8257536 | tf_op jit(solution)/shard_map/dot_general | solution.py:23
  189.8 35.4 %all-reduce.3.cloned.1.call-done = f32[256,1024]{1,0:T(8,128)} async-done(((f32[256,1024]{1,0:T(8,128)}), f32[256,1024]{1,0:T(8,128)}) %all-reduce.3.cloned.1.call-update) | async-done | bytes 1048592 | tf_op jit(solution)/shard_map/psum | solution.py:26
  225.2 1.5 fusion.3
  226.7 0.8 copy.12
  227.6 5.9 %fusion.8 = f32[256,2816]{1,0:T(8,128)} fusion(bf16[1024,2816]{1,0:T(8,128)(2,1)} %param.15, bf16[256,1024]{1,0:T(8,128)(2,1)S(1)} %get-tuple-element.6, f32[1024]{0:T(1024)S(1)} %convert_element_type.36), kind=kOutput, calls=%fused_computation.15 | convolution fusion | flops 1477181440 | bytes 9179136 | tf_op jit(solution)/shard_map/dot_general | solution.py:14
  233.5 5.9 %fusion.6 = f32[256,2816]{1,0:T(8,128)} fusion(bf16[1024,2816]{1,0:T(8,128)(2,1)} %param.16, bf16[256,1024]{1,0:T(8,128)(2,1)S(1)} %get-tuple-element.6, f32[1024]{0:T(1024)S(1)} %convert_element_type.36), kind=kOutput, calls=%fused_computation.14 | convolution fusion | flops 1477181440 | bytes 9179136 | tf_op jit(solution)/shard_map/dot_general | solution.py:15
  239.6 8.1 %reduce-scatter.21.cloned.1.call-done = f32[64,1]{1,0:T(8,128)} async-done(((f32[256,1]{1,0:T(8,128)}), f32[64,1]{1,0:T(8,128)}) %reduce-scatter.21.cloned.1.call-update) | async-done | bytes 272
  247.6 0.8 add_rsqrt_fusion
  248.4 0.1 copy.15
  248.5 56.0 %reduce-scatter.15.cloned.1.call-done = f32[64,2816]{1,0:T(8,128)} async-done(((f32[256,2816]{1,0:T(8,128)}), f32[64,2816]{1,0:T(8,128)}) %reduce-scatter.15.cloned.1.call-update) | async-done | bytes 720912 | tf_op jit(solution)/shard_map/reduce_scatter | solution.py:17
  304.4 58.4 %reduce-scatter.17.cloned.1.call-done = f32[64,2816]{1,0:T(8,128)} async-done(((f32[256,2816]{1,0:T(8,128)}), f32[64,2816]{1,0:T(8,128)}) %reduce-scatter.17.cloned.1.call-update) | async-done | bytes 720912 | tf_op jit(solution)/shard_map/reduce_scatter | solution.py:18
  362.9 2.3 multiply_convert_fusion
  365.2 0.0 all-reduce.5.cloned.1.call-start
  365.3 34.6 %all-gather.5.cloned.1.call-done = bf16[256,2816]{1,0:T(8,128)(2,1)} async-done(((bf16[64,2816]{1,0:T(8,128)(2,1)}), bf16[256,2816]{1,0:T(8,128)(2,1)}) %all-gather.5.cloned.1.call-update) | async-done | bytes 1441808 | tf_op jit(solution)/shard_map/all_gather | solution.py:24
  399.9 5.7 %fusion.16 = f32[256,1024]{1,0:T(8,128)} fusion(bf16[256,2816]{1,0:T(8,128)(2,1)} %all-gather.5.cloned.1.call-done, bf16[2816,1024]{1,0:T(8,128)(2,1)} %param.17), kind=kOutput, calls=%fused_computation.21 | convolution fusion | flops 1476395008 | bytes 8257536 | tf_op jit(solution)/shard_map/dot_general | solution.py:23
  405.6 35.4 %all-reduce.5.cloned.1.call-done = f32[256,1024]{1,0:T(8,128)} async-done(((f32[256,1024]{1,0:T(8,128)}), f32[256,1024]{1,0:T(8,128)}) %all-reduce.5.cloned.1.call-update) | async-done | bytes 1048592 | tf_op jit(solution)/shard_map/psum | solution.py:26
  441.0 2.2 fusion.5
  (21 shorter events, 0.4 us)
Async XLA Ops:
  6.5 25.2 %reduce-scatter.19.cloned.1.call-start = ((), (), s32[]{:S(2)}) async-start(), calls=%async_computation.14 | async-start | bytes 163840
  8.6 80.0 %reduce-scatter.13.cloned.1.call-start = ((), (), s32[]{:S(2)}) async-start(), calls=%async_computation.7 | async-start | bytes 3604480 | tf_op jit(solution)/shard_map/reduce_scatter | solution.py:18
  9.3 6.2 %copy-start = (bf16[256,1024]{1,0:T(8,128)(2,1)S(1)}, bf16[256,1024]{1,0:T(8,128)(2,1)}, u32[]{:S(2)}) copy-start(bf16[256,1024]{1,0:T(8,128)(2,1)} %param.9) | copy-start | bytes 1572868
  15.4 131.6 %reduce-scatter.11.cloned.1.call-start = ((), (), s32[]{:S(2)}) async-start(), calls=%async_computation.6 | async-start | bytes 3604480 | tf_op jit(solution)/shard_map/reduce_scatter | solution.py:17
  21.5 162.6 %all-gather.3.cloned.1.call-start = ((), (), s32[]{:S(2)}) async-start(), calls=%async_computation.8 | async-start | bytes 1802240 | tf_op jit(solution)/shard_map/all_gather | solution.py:24
  149.4 40.4 %copy-start.1 = (bf16[1024]{0:T(1024)(128)(2,1)S(1)}, bf16[1024]{0:T(1024)(128)(2,1)}, u32[]{:S(2)}) copy-start(bf16[1024]{0:T(1024)(128)(2,1)} %param.14) | copy-start | bytes 6148
  149.4 75.8 %all-reduce.3.cloned.1.call-start = ((), (), s32[]{:S(2)}) async-start(), calls=%async_computation.9 | async-start | bytes 2097152 | tf_op jit(solution)/shard_map/psum | solution.py:26
  189.8 57.9 %reduce-scatter.21.cloned.1.call-start = ((), (), s32[]{:S(2)}) async-start(), calls=%async_computation.15 | async-start | bytes 163840
  227.5 76.9 %reduce-scatter.15.cloned.1.call-start = ((), (), s32[]{:S(2)}) async-start(), calls=%async_computation.10 | async-start | bytes 3604480 | tf_op jit(solution)/shard_map/reduce_scatter | solution.py:17
  233.5 129.4 %reduce-scatter.17.cloned.1.call-start = ((), (), s32[]{:S(2)}) async-start(), calls=%async_computation.11 | async-start | bytes 3604480 | tf_op jit(solution)/shard_map/reduce_scatter | solution.py:18
  239.5 160.4 %all-gather.5.cloned.1.call-start = ((), (), s32[]{:S(2)}) async-start(), calls=%async_computation.12 | async-start | bytes 1802240 | tf_op jit(solution)/shard_map/all_gather | solution.py:24
  365.2 75.8 %all-reduce.5.cloned.1.call-start = ((), (), s32[]{:S(2)}) async-start(), calls=%async_computation.13 | async-start | bytes 2097152 | tf_op jit(solution)/shard_map/psum | solution.py:26
Sparse Core Ops, SparseCore 0:
  9.6 22.1 reduce-scatter.18
  34.1 54.4 reduce-scatter.12
  90.9 56.0 reduce-scatter.10
  149.5 34.5 all-gather.2
  189.9 35.2 all-reduce.2
  227.6 19.9 reduce-scatter.20
  249.9 54.4 reduce-scatter.14
  306.7 56.0 reduce-scatter.16
  365.3 34.5 all-gather.4
  405.7 35.2 all-reduce.4
where the time goes:
time: 451 us; the launch traced here: 450 us
  waiting for transfers between devices  387 us (86%)
  matrix products  35.2 us (8%)
  between operations  13.6 us (3%)
  other arithmetic  11.8 us (3%)
    reduce_scatter x2, waiting for transfers between devices, half_step(): lax.psum_scatter(up_part, 'ra', scatter_dimension=0, tiled=True)  114 us
    reduce_scatter x2, waiting for transfers between devices, half_step(): lax.psum_scatter(gate_part, 'ra', scatter_dimension=0, tiled=True)  114 us
    psum x2, waiting for transfers between devices, half_step(): branch = lax.psum(down_part, 'cb')  70.8 us
    all_gather x2, waiting for transfers between devices, half_step(): lax.all_gather(hidden, 'ra', axis=0, tiled=True)  69.2 us
    unnamed x12, waiting for transfers between devices  18.5 us
    dot_general x2, matrix products, half_step(): up_part = jnp.dot(normed, w_up, preferred_element_type=jnp.float32)  12 us
    dot_general x2, matrix products, half_step(): gate_part = jnp.dot(normed, w_gate, preferred_element_type=jnp.float32)  11.8 us
    dot_general x2, matrix products, half_step(): jnp.dot(lax.all_gather(hidden, 'ra', axis=0, tiled=True), w_down, preferr...  11.4 us
  transfers between devices with their start and end apart: 10, of which 10 were waited for; matrix products, arithmetic and copies ran while one was open for 6% of the time, Pallas kernels for 0%

commit v1 on v0

--- a/solution.py
+++ b/solution.py
@@ -23,7 +23,7 @@
     down_part = jnp.dot(
         lax.all_gather(hidden, "ra", axis=0, tiled=True), w_down, preferred_element_type=jnp.float32
     )
-    branch = lax.psum(down_part, "cb")
+    branch = jnp.sum(lax.all_gather(down_part, "cb"), axis=0)
     return (values + 0.5 * branch).astype(jnp.bfloat16)
 
 

time: 451 us -> 450 us (level)
    psum x2 -> x0, waiting for transfers between devices: 70.8 us -> none  [half_step(): branch = lax.psum(down_part, 'cb')]
    all_gather x0 -> x2, waiting for transfers between devices: none -> 67.1 us  [half_step(): branch = jnp.sum(lax.all_gather(down_part, 'cb'), axis=0)]
    reduce_sum x0 -> x2, other arithmetic: none -> 5.44 us  [half_step(): branch = jnp.sum(lax.all_gather(down_part, 'cb'), axis=0)]
where the time goes in v1:
time: 450 us; the launch traced here: 449 us
  waiting for transfers between devices  383 us (85%)
  matrix products  35.3 us (8%)
  other arithmetic  14.8 us (3%)
  between operations  13.6 us (3%)
    reduce_scatter x2, waiting for transfers between devices, half_step(): lax.psum_scatter(up_part, 'ra', scatter_dimension=0, tiled=True)  114 us
    reduce_scatter x2, waiting for transfers between devices, half_step(): lax.psum_scatter(gate_part, 'ra', scatter_dimension=0, tiled=True)  114 us
    all_gather x2, waiting for transfers between devices, half_step(): lax.all_gather(hidden, 'ra', axis=0, tiled=True)  69.2 us
    all_gather x2, waiting for transfers between devices, half_step(): branch = jnp.sum(lax.all_gather(down_part, 'cb'), axis=0)  67.1 us
    unnamed x12, waiting for transfers between devices  18 us
    dot_general x2, matrix products, half_step(): up_part = jnp.dot(normed, w_up, preferred_element_type=jnp.float32)  12 us
    dot_general x2, matrix products, half_step(): gate_part = jnp.dot(normed, w_gate, preferred_element_type=jnp.float32)  11.8 us
    dot_general x2, matrix products, half_step(): jnp.dot(lax.all_gather(hidden, 'ra', axis=0, tiled=True), w_down, preferr...  11.4 us
  transfers between devices with their start and end apart: 10, of which 10 were waited for; matrix products, arithmetic and copies ran while one was open for 6% of the time, Pallas kernels for 0%

profile of v1, /device:TPU:0, one launch (start us, length us, event | category | flops | bytes accessed | tf_op | source)
XLA Modules:
  0.0 448.9 jit_solution(3726252501181231483)
XLA Ops:
  6.5 1.2 fusion
  7.8 0.8 copy.10
  8.6 0.0 reduce-scatter.13.cloned.1.call-start
  8.6 0.7 convert_element_type.31
  9.3 6.1 %fusion.10 = f32[256,2816]{1,0:T(8,128)} fusion(bf16[1024,2816]{1,0:T(8,128)(2,1)} %param.12, bf16[256,1024]{1,0:T(8,128)(2,1)} %param.9, f32[1024]{0:T(1024)S(1)} %convert_element_type.31), kind=kOutput, calls=%fused_computation.16 | convolution fusion | flops 1477181440 | bytes 9179136 | tf_op jit(solution)/shard_map/dot_general | solution.py:15
  15.4 0.0 reduce-scatter.11.cloned.1.call-start
  15.5 5.9 %fusion.12 = f32[256,2816]{1,0:T(8,128)} fusion(bf16[1024,2816]{1,0:T(8,128)(2,1)} %param.11, bf16[256,1024]{1,0:T(8,128)(2,1)S(1)} %copy-done, f32[1024]{0:T(1024)S(1)} %convert_element_type.31), kind=kOutput, calls=%fused_computation.17 | convolution fusion | flops 1477181440 | bytes 9179136 | tf_op jit(solution)/shard_map/dot_general | solution.py:14
  21.5 10.3 %reduce-scatter.19.cloned.1.call-done = f32[64,1]{1,0:T(8,128)} async-done(((f32[256,1]{1,0:T(8,128)}), f32[64,1]{1,0:T(8,128)}) %reduce-scatter.19.cloned.1.call-update) | async-done | bytes 272
  31.8 0.8 add_rsqrt_fusion.1
  32.5 0.1 copy.14
  32.6 56.0 %reduce-scatter.13.cloned.1.call-done = f32[64,2816]{1,0:T(8,128)} async-done(((f32[256,2816]{1,0:T(8,128)}), f32[64,2816]{1,0:T(8,128)}) %reduce-scatter.13.cloned.1.call-update) | async-done | bytes 720912 | tf_op jit(solution)/shard_map/reduce_scatter | solution.py:18
  88.6 58.4 %reduce-scatter.11.cloned.1.call-done = f32[64,2816]{1,0:T(8,128)} async-done(((f32[256,2816]{1,0:T(8,128)}), f32[64,2816]{1,0:T(8,128)}) %reduce-scatter.11.cloned.1.call-update) | async-done | bytes 720912 | tf_op jit(solution)/shard_map/reduce_scatter | solution.py:17
  147.0 2.3 multiply_convert_fusion.1
  149.4 34.6 %all-gather.7.cloned.1.call-done = bf16[256,2816]{1,0:T(8,128)(2,1)} async-done(((bf16[64,2816]{1,0:T(8,128)(2,1)}), bf16[256,2816]{1,0:T(8,128)(2,1)}) %all-gather.7.cloned.1.call-update) | async-done | bytes 1441808 | tf_op jit(solution)/shard_map/all_gather | solution.py:24
  184.1 5.7 %fusion.15 = f32[256,1024]{1,0:T(8,128)} fusion(bf16[256,2816]{1,0:T(8,128)(2,1)} %all-gather.7.cloned.1.call-done, bf16[2816,1024]{1,0:T(8,128)(2,1)} %param.13), kind=kOutput, calls=%fused_computation.20 | convolution fusion | flops 1476395008 | bytes 8257536 | tf_op jit(solution)/shard_map/dot_general | solution.py:23
  189.9 33.5 %all-gather.11.cloned.1.call-done = f32[1024,1024]{1,0:T(8,128)} async-done(((f32[256,1024]{1,0:T(8,128)}), f32[1024,1024]{1,0:T(8,128)}) %all-gather.11.cloned.1.call-update) | async-done | bytes 4194320 | tf_op jit(solution)/shard_map/all_gather | solution.py:26
  223.4 2.7 reduce_sum.37
  226.1 0.3 fusion.3
  226.4 0.8 copy.12
  227.3 5.9 %fusion.8 = f32[256,2816]{1,0:T(8,128)} fusion(bf16[1024,2816]{1,0:T(8,128)(2,1)} %param.15, bf16[256,1024]{1,0:T(8,128)(2,1)S(1)} %get-tuple-element.6, f32[1024]{0:T(1024)S(1)} %convert_element_type.36), kind=kOutput, calls=%fused_computation.15 | convolution fusion | flops 1477181440 | bytes 9179136 | tf_op jit(solution)/shard_map/dot_general | solution.py:14
  233.2 5.9 %fusion.6 = f32[256,2816]{1,0:T(8,128)} fusion(bf16[1024,2816]{1,0:T(8,128)(2,1)} %param.16, bf16[256,1024]{1,0:T(8,128)(2,1)S(1)} %get-tuple-element.6, f32[1024]{0:T(1024)S(1)} %convert_element_type.36), kind=kOutput, calls=%fused_computation.14 | convolution fusion | flops 1477181440 | bytes 9179136 | tf_op jit(solution)/shard_map/dot_general | solution.py:15
  239.2 7.6 %reduce-scatter.21.cloned.1.call-done = f32[64,1]{1,0:T(8,128)} async-done(((f32[256,1]{1,0:T(8,128)}), f32[64,1]{1,0:T(8,128)}) %reduce-scatter.21.cloned.1.call-update) | async-done | bytes 272
  246.8 0.8 add_rsqrt_fusion
  247.6 0.1 copy.15
  247.7 56.0 %reduce-scatter.15.cloned.1.call-done = f32[64,2816]{1,0:T(8,128)} async-done(((f32[256,2816]{1,0:T(8,128)}), f32[64,2816]{1,0:T(8,128)}) %reduce-scatter.15.cloned.1.call-update) | async-done | bytes 720912 | tf_op jit(solution)/shard_map/reduce_scatter | solution.py:17
  303.7 58.4 %reduce-scatter.17.cloned.1.call-done = f32[64,2816]{1,0:T(8,128)} async-done(((f32[256,2816]{1,0:T(8,128)}), f32[64,2816]{1,0:T(8,128)}) %reduce-scatter.17.cloned.1.call-update) | async-done | bytes 720912 | tf_op jit(solution)/shard_map/reduce_scatter | solution.py:18
  362.1 2.3 multiply_convert_fusion
  364.5 34.6 %all-gather.9.cloned.1.call-done = bf16[256,2816]{1,0:T(8,128)(2,1)} async-done(((bf16[64,2816]{1,0:T(8,128)(2,1)}), bf16[256,2816]{1,0:T(8,128)(2,1)}) %all-gather.9.cloned.1.call-update) | async-done | bytes 1441808 | tf_op jit(solution)/shard_map/all_gather | solution.py:24
  399.1 5.7 %fusion.16 = f32[256,1024]{1,0:T(8,128)} fusion(bf16[256,2816]{1,0:T(8,128)(2,1)} %all-gather.9.cloned.1.call-done, bf16[2816,1024]{1,0:T(8,128)(2,1)} %param.17), kind=kOutput, calls=%fused_computation.21 | convolution fusion | flops 1476395008 | bytes 8257536 | tf_op jit(solution)/shard_map/dot_general | solution.py:23
  404.8 33.6 %all-gather.13.cloned.1.call-done = f32[1024,1024]{1,0:T(8,128)} async-done(((f32[256,1024]{1,0:T(8,128)}), f32[1024,1024]{1,0:T(8,128)}) %all-gather.13.cloned.1.call-update) | async-done | bytes 4194320 | tf_op jit(solution)/shard_map/all_gather | solution.py:26
  438.4 2.7 reduce_sum.39
  441.2 1.0 fusion.5
  (23 shorter events, 0.5 us)
Async XLA Ops:
  6.5 25.2 %reduce-scatter.19.cloned.1.call-start = ((), (), s32[]{:S(2)}) async-start(), calls=%async_computation.14 | async-start | bytes 163840
  8.6 80.0 %reduce-scatter.13.cloned.1.call-start = ((), (), s32[]{:S(2)}) async-start(), calls=%async_computation.7 | async-start | bytes 3604480 | tf_op jit(solution)/shard_map/reduce_scatter | solution.py:18
  9.3 6.2 %copy-start = (bf16[256,1024]{1,0:T(8,128)(2,1)S(1)}, bf16[256,1024]{1,0:T(8,128)(2,1)}, u32[]{:S(2)}) copy-start(bf16[256,1024]{1,0:T(8,128)(2,1)} %param.9) | copy-start | bytes 1572868
  15.4 131.6 %reduce-scatter.11.cloned.1.call-start = ((), (), s32[]{:S(2)}) async-start(), calls=%async_computation.6 | async-start | bytes 3604480 | tf_op jit(solution)/shard_map/reduce_scatter | solution.py:17
  21.5 162.6 %all-gather.7.cloned.1.call-start = ((), (), s32[]{:S(2)}) async-start(), calls=%async_computation.8 | async-start | bytes 1802240 | tf_op jit(solution)/shard_map/all_gather | solution.py:24
  149.4 40.5 %copy-start.1 = (bf16[1024]{0:T(1024)(128)(2,1)S(1)}, bf16[1024]{0:T(1024)(128)(2,1)}, u32[]{:S(2)}) copy-start(bf16[1024]{0:T(1024)(128)(2,1)} %param.14) | copy-start | bytes 6148
  149.4 74.0 %all-gather.11.cloned.1.call-start = ((), (), s32[]{:S(2)}) async-start(), calls=%async_computation.12 | async-start | bytes 5242880 | tf_op jit(solution)/shard_map/all_gather | solution.py:26
  189.8 57.0 %reduce-scatter.21.cloned.1.call-start = ((), (), s32[]{:S(2)}) async-start(), calls=%async_computation.15 | async-start | bytes 163840
  227.2 76.4 %reduce-scatter.15.cloned.1.call-start = ((), (), s32[]{:S(2)}) async-start(), calls=%async_computation.9 | async-start | bytes 3604480 | tf_op jit(solution)/shard_map/reduce_scatter | solution.py:17
  233.2 128.9 %reduce-scatter.17.cloned.1.call-start = ((), (), s32[]{:S(2)}) async-start(), calls=%async_computation.10 | async-start | bytes 3604480 | tf_op jit(solution)/shard_map/reduce_scatter | solution.py:18
  239.2 159.9 %all-gather.9.cloned.1.call-start = ((), (), s32[]{:S(2)}) async-start(), calls=%async_computation.11 | async-start | bytes 1802240 | tf_op jit(solution)/shard_map/all_gather | solution.py:24
  364.4 74.0 %all-gather.13.cloned.1.call-start = ((), (), s32[]{:S(2)}) async-start(), calls=%async_computation.13 | async-start | bytes 5242880 | tf_op jit(solution)/shard_map/all_gather | solution.py:26
Sparse Core Ops, SparseCore 0:
  9.6 22.1 reduce-scatter.18
  34.1 54.4 reduce-scatter.12
  90.9 56.0 reduce-scatter.10
  149.5 34.5 all-gather.6
  189.9 33.4 all-gather.10
  227.3 19.4 reduce-scatter.20
  249.1 54.4 reduce-scatter.14
  306.0 56.0 reduce-scatter.16
  364.5 34.5 all-gather.8
  405.0 33.4 all-gather.12
